TPU v7x, 32 devices: a whole 2x2x4 slice. The times are simulated.
32 devices in a mesh: sp: 16 (over z, y, core), tp: 2 (over x).
Axes of the slice: x: 2, y: 2, z: 4, core: 2. Of those that a mesh axis runs over, the one named last changes fastest.
Arguments:
- residual: bfloat16 [2048, 2048], P(('sp', 'tp')), may hold values from -6 to 6
- q_small: bfloat16 [2048, 1024], P('sp', 'tp'), may hold values from -6 to 6
- k_small: bfloat16 [2048, 1024], P('sp', 'tp'), may hold values from -6 to 6
- v_small: bfloat16 [2048, 1024], P('sp', 'tp'), may hold values from -6 to 6
- q_large: bfloat16 [2048, 1024], P('sp', 'tp'), may hold values from -6 to 6
- k_large: bfloat16 [2048, 1024], P('sp', 'tp'), may hold values from -6 to 6
- v_large: bfloat16 [2048, 1024], P('sp', 'tp'), may hold values from -6 to 6
- forget_small: float32 [2048, 16], P('sp', 'tp'), may hold values from 0 to 20
- forget_large: float32 [2048, 8], P('sp', 'tp'), may hold values from 0 to 20
- w_out_small: bfloat16 [1024, 2048], P('tp'), may hold values from -0.125 to 0.125
- w_out_large: bfloat16 [1024, 2048], P('tp'), may hold values from -0.125 to 0.125
- norm_gain: float32 [2048], replicated, may hold values from 0.1 to 1.9
- w_gate: bfloat16 [2048, 4096], P('sp', 'tp'), may hold values from -0.125 to 0.125
- w_up: bfloat16 [2048, 4096], P('sp', 'tp'), may hold values from -0.125 to 0.125
- conv_gate: float32 [3, 4096], P(None, 'tp'), may hold values from -3 to 3
- conv_up: float32 [3, 4096], P(None, 'tp'), may hold values from -3 to 3
- w_down: bfloat16 [4096, 2048], P('tp', 'sp'), may hold values from -0.09375 to 0.09375
Outputs:
- mixed: bfloat16 [2048, 2048], P(('sp', 'tp'))
All inputs are finite; a program needn't handle non-finite values.
Results may differ from a plain program's by a relative error of at most 0.015.
Values may be sent and summed in bfloat16 or wider, within the bound.
A program may use at most 64 MiB of HBM per device.

v0:
```python
import jax
import jax.numpy as jnp
from jax import lax
from jax.sharding import PartitionSpec as P

EPS = 1e-06
NEG = -1e30


def from_behind(block, axis, distance):
    devices = range(lax.axis_size(axis))
    route = [(i - distance, i) for i in devices if i - distance in devices]
    return lax.ppermute(block, axis, route)


def globalize(part, rows):
    heads = part.shape[1]
    blocks = part.reshape(-1, rows, heads)
    totals = blocks[:, -1, :]
    before = jnp.cumsum(totals, axis=0) - totals
    return (blocks + before[:, None, :]).reshape(part.shape)


def attend(carry, keys, values, queries, cum_own, cum_every, qpos):
    top, denom, accum = carry
    count = keys.shape[0]
    heads = queries.shape[1]
    size = queries.shape[2]
    keys = keys.reshape(count, heads, size)
    values = values.reshape(count, heads, size)
    kpos = jnp.arange(count, dtype=jnp.int32)
    scores = jnp.einsum(
        "qhd,khd->qhk", queries, keys, preferred_element_type=jnp.float32
    ) * size ** (-0.5)
    scores = scores + cum_own[:, :, None] - cum_every.T[None, :, :]
    keep = (kpos[None, :] <= qpos[:, None])[:, None, :]
    scores = jnp.where(keep, scores, NEG)
    new_top = jnp.maximum(top, jnp.max(scores, axis=-1))
    weights = jnp.where(keep, jnp.exp(scores - new_top[:, :, None]), 0.0)
    denom = jnp.sum(weights, axis=-1)
    accum = jnp.einsum(
        "qhk,khd->qhd", weights.astype(jnp.bfloat16), values, preferred_element_type=jnp.float32
    )
    return (new_top, denom, accum)


def finish(carry):
    top, denom, accum = carry
    attended = accum / denom[:, :, None]
    normed = attended * lax.rsqrt(jnp.mean(attended * attended, axis=-1, keepdims=True) + EPS)
    return normed.astype(jnp.bfloat16).reshape(attended.shape[0], -1)


def empty_carry(rows, heads, size):
    return (
        jnp.full((rows, heads), NEG, jnp.float32),
        jnp.zeros((rows, heads), jnp.float32),
        jnp.zeros((rows, heads, size), jnp.float32),
    )


def body(
    residual,
    q_small,
    k_small,
    v_small,
    q_large,
    k_large,
    v_large,
    forget_small,
    forget_large,
    w_out_small,
    w_out_large,
    norm_gain,
    w_gate,
    w_up,
    conv_gate,
    conv_up,
    w_down,
):
    rows = q_small.shape[0]
    offset = lax.axis_index("sp") * rows
    qpos = offset + jnp.arange(rows, dtype=jnp.int32)
    gathered = (
        lax.all_gather(w_gate, "sp", axis=0, tiled=True),
        lax.all_gather(w_up, "sp", axis=0, tiled=True),
        lax.all_gather(w_down, "sp", axis=1, tiled=True),
    )
    local_small = jnp.cumsum(jax.nn.log_sigmoid(forget_small), axis=0)
    local_large = jnp.cumsum(jax.nn.log_sigmoid(forget_large), axis=0)
    part_small, part_large = (
        lax.all_gather(local_small, "sp", axis=0, tiled=True),
        lax.all_gather(local_large, "sp", axis=0, tiled=True),
    )
    every_small = globalize(part_small, rows)
    every_large = globalize(part_large, rows)
    cum_small = lax.dynamic_slice_in_dim(every_small, offset, rows, 0)
    cum_large = lax.dynamic_slice_in_dim(every_large, offset, rows, 0)
    heads_small = forget_small.shape[1]
    heads_large = forget_large.shape[1]
    queries_small = q_small.reshape(rows, heads_small, -1)
    queries_large = q_large.reshape(rows, heads_large, -1)
    start_carry = (
        empty_carry(rows, heads_small, queries_small.shape[2]),
        empty_carry(rows, heads_large, queries_large.shape[2]),
    )
    keys_s = lax.all_gather(k_small, "sp", axis=0, tiled=True)
    values_s = lax.all_gather(v_small, "sp", axis=0, tiled=True)
    keys_l = lax.all_gather(k_large, "sp", axis=0, tiled=True)
    values_l = lax.all_gather(v_large, "sp", axis=0, tiled=True)
    small = attend(start_carry[0], keys_s, values_s, queries_small, cum_small, every_small, qpos)
    large = attend(start_carry[1], keys_l, values_l, queries_large, cum_large, every_large, qpos)
    normed_small = finish(small)
    normed_large = finish(large)
    first_part = jnp.dot(normed_small, w_out_small, preferred_element_type=jnp.float32)
    projected = lax.psum_scatter(
        (
            first_part + jnp.dot(normed_large, w_out_large, preferred_element_type=jnp.float32)
        ).astype(jnp.bfloat16),
        "tp",
        scatter_dimension=0,
        tiled=True,
    ).astype(jnp.float32)
    first = residual.astype(jnp.float32) + projected
    normal = (
        first * lax.rsqrt(jnp.mean(first * first, axis=-1, keepdims=True) + EPS) * norm_gain
    ).astype(jnp.bfloat16)
    gate_full, up_full, down_full = gathered
    piece = lax.all_gather(normal, "tp", axis=0, tiled=True)
    gate_part = jnp.dot(piece, gate_full, preferred_element_type=jnp.float32).astype(jnp.bfloat16)
    up_part = jnp.dot(piece, up_full, preferred_element_type=jnp.float32).astype(jnp.bfloat16)
    both = jnp.concatenate([gate_part, up_part], axis=1)
    width = both.shape[0]
    rim = from_behind(both[width - 2 :], "sp", 1)
    extended = jnp.concatenate([rim, both], axis=0).astype(jnp.float32)
    taps = jnp.concatenate([conv_gate, conv_up], axis=1)
    conv = (
        taps[0] * extended[0:width]
        + taps[1] * extended[1 : width + 1]
        + taps[2] * extended[2 : width + 2]
    )
    half = gate_full.shape[1]
    hidden = (jax.nn.silu(conv[:, :half]) * conv[:, half:]).astype(jnp.bfloat16)
    mixed = first + lax.psum_scatter(
        jnp.dot(hidden, down_full, preferred_element_type=jnp.float32).astype(jnp.bfloat16),
        "tp",
        scatter_dimension=0,
        tiled=True,
    ).astype(jnp.float32)
    return mixed.astype(jnp.bfloat16)


def solution(mesh):
    placed = (
        P(("sp", "tp"), None),
        P("sp", "tp"),
        P("sp", "tp"),
        P("sp", "tp"),
        P("sp", "tp"),
        P("sp", "tp"),
        P("sp", "tp"),
        P("sp", "tp"),
        P("sp", "tp"),
        P("tp", None),
        P("tp", None),
        P(),
        P("sp", "tp"),
        P("sp", "tp"),
        P(None, "tp"),
        P(None, "tp"),
        P("tp", "sp"),
    )
    return jax.shard_map(
        body, mesh=mesh, in_specs=placed, out_specs=P(("sp", "tp"), None), check_vma=False
    )
```

profile of v0, /device:TPU:0, one launch (start us, length us, event | category | flops | bytes accessed | tf_op | source)
XLA Modules:
  0.0 472.0 jit_solution(16428870450614130786)
XLA Ops:
  8.1 1.7 copy.44
  11.4 27.1 %all_gather.34 = f32[2048,4]{1,0:T(8,128)S(1)} all-gather(f32[128,4]{1,0:T(8,128)S(1)} %reduce_window_sum.46), channel_id=1, replica_groups=mesh['sp'=16,'tp'=2] {'sp'}, dimensions={0}, use_global_device_ids=true | all-gather | bytes 34816 | tf_op jit(solution)/shard_map/all_gather | solution.py:93
  38.8 24.5 %all_gather.31 = f32[2048,8]{1,0:T(8,128)S(1)} all-gather(f32[128,8]{1,0:T(8,128)S(1)} %reduce_window_sum.44), channel_id=1, replica_groups=mesh['sp'=16,'tp'=2] {'sp'}, dimensions={0}, use_global_device_ids=true | all-gather | bytes 69632 | tf_op jit(solution)/shard_map/all_gather | solution.py:92
  63.4 1.1 bitcast_add_fusion.3
  65.7 1.6 copy.41
  67.7 4.0 copy.52
  71.7 31.4 %all-gather.8.cloned.1.call-done = bf16[2048,512]{1,0:T(8,128)(2,1)} async-done(((bf16[128,512]{1,0:T(8,128)(2,1)}), bf16[2048,512]{1,0:T(8,128)(2,1)}) %all-gather.8.cloned.1.call-update) | async-done | bytes 2097168 | tf_op jit(solution)/shard_map/all_gather | solution.py:107
  103.0 4.0 copy.35
  107.0 38.0 %all-gather.12.cloned.1.call-done = bf16[2048,512]{0,1:T(8,128)(2,1)} async-done(((bf16[128,512]{0,1:T(8,128)(2,1)}), bf16[2048,512]{0,1:T(8,128)(2,1)}) %all-gather.12.cloned.1.call-update) | async-done | bytes 2097168 | tf_op jit(solution)/shard_map/all_gather | solution.py:109
  145.0 3.7 fusion.47
  150.3 1.2 multiply_reduce_fusion.1
  151.9 3.4 fusion.4
  155.3 3.2 copy-done.2
  158.5 3.1 fusion.2
  161.6 26.0 %all-gather.10.cloned.1.call-done = bf16[2048,512]{1,0:T(8,128)(2,1)} async-done(((bf16[128,512]{1,0:T(8,128)(2,1)}), bf16[2048,512]{1,0:T(8,128)(2,1)}) %all-gather.10.cloned.1.call-update) | async-done | bytes 2097168 | tf_op jit(solution)/shard_map/all_gather | solution.py:108
  187.6 3.9 copy.42
  191.5 6.6 %multiply_reduce_fusion.2 = (f32[128,8]{0,1:T(8,128)S(1)}, f32[128,8,64]{0,2,1:T(8,128)S(1)}) fusion(f32[128,8]{0,1:T(8,128)S(1)} %fusion.2, bf16[2048,8,64]{0,2,1:T(8,128)(2,1)} %bitcast.82, f32[8,2048,128]{2,1,0:T(8,128)} %copy-done.2, f32[128,8]{0,1:T(8,128)S(1)} %broadcast_maximum_fusion, f32[8,2048]{1,0:T(8,128)S(1)} %copy.41, f32[128,8]{0,1:T(8,128)S(1)} %copy.40, ...), kind=kOutput, calls=%fused_computation.49 | convolution fusion | flops 283311104 | bytes 11091968 | tf_op jit(solution)/shard_map/qhk,khd->qhd/dot_general | solution.py:41
  199.7 1.3 fusion.12
  203.2 11.3 %reduce-scatter.3.cloned.1.call-done = bf16[64,2048]{1,0:T(8,128)(2,1)} async-done(((bf16[128,2048]{1,0:T(8,128)(2,1)}), bf16[64,2048]{1,0:T(8,128)(2,1)}) %reduce-scatter.3.cloned.1.call-update) | async-done | bytes 262160 | tf_op jit(solution)/shard_map/reduce_scatter | solution.py:116
  214.6 1.1 multiply_reduce_fusion
  215.7 1.1 multiply_convert_fusion
  216.8 8.7 %all_gather.36 = bf16[128,2048]{1,0:T(8,128)(2,1)S(1)} all-gather(bf16[64,2048]{1,0:T(8,128)(2,1)S(1)} %multiply_convert_fusion), channel_id=1, replica_groups=mesh['sp'=16,'tp'=2] {'tp'}, dimensions={0}, use_global_device_ids=true | all-gather | bytes 786432 | tf_op jit(solution)/shard_map/all_gather | solution.py:129
  225.5 65.4 %all-gather.18.cloned.1.call-done = bf16[2048,2048]{1,0:T(8,128)(2,1)} async-done(((bf16[128,2048]{1,0:T(8,128)(2,1)}), bf16[2048,2048]{1,0:T(8,128)(2,1)}) %all-gather.18.cloned.1.call-update) | async-done | bytes 8388624 | tf_op jit(solution)/shard_map/all_gather | solution.py:86
  290.9 4.6 convolution_convert_fusion.1
  295.6 70.4 %all-gather.16.cloned.1.call-done = bf16[2048,2048]{1,0:T(8,128)(2,1)} async-done(((bf16[128,2048]{1,0:T(8,128)(2,1)}), bf16[2048,2048]{1,0:T(8,128)(2,1)}) %all-gather.16.cloned.1.call-update) | async-done | bytes 8388624 | tf_op jit(solution)/shard_map/all_gather | solution.py:85
  366.0 4.6 convolution_convert_fusion.2
  370.7 2.2 collective-permute-start
  373.9 2.0 fusion.15
  375.9 68.5 %all-gather.20.cloned.1.call-done = bf16[2048,2048]{1,0:T(8,128)(2,1)} async-done(((bf16[2048,128]{1,0:T(8,128)(2,1)}), bf16[2048,2048]{1,0:T(8,128)(2,1)}) %all-gather.20.cloned.1.call-update) | async-done | bytes 8388624 | tf_op jit(solution)/shard_map/all_gather | solution.py:87
  444.5 6.3 %convolution_convert_fusion = bf16[128,2048]{1,0:T(8,128)(2,1)} fusion(bf16[2048,2048]{1,0:T(8,128)(2,1)} %all-gather.20.cloned.1.call-done, f32[128,4096]{1,0:T(8,128)} %fusion.15), kind=kOutput, calls=%fused_computation.16 | convolution fusion | flops 1075576832 | bytes 11010048 | tf_op jit(solution)/shard_map/dot_general | solution.py:145
  450.8 13.0 %reduce-scatter.5.cloned.1.call-done = bf16[64,2048]{1,0:T(8,128)(2,1)} async-done(((bf16[128,2048]{1,0:T(8,128)(2,1)}), bf16[64,2048]{1,0:T(8,128)(2,1)}) %reduce-scatter.5.cloned.1.call-update) | async-done | bytes 262160 | tf_op jit(solution)/shard_map/reduce_scatter | solution.py:144
  463.8 1.7 add_convert_fusion
  (78 shorter events, 12.0 us)
Async XLA Ops:
  6.5 191.7 %copy-start = (bf16[512,2048]{1,0:T(8,128)(2,1)S(1)}, bf16[512,2048]{1,0:T(8,128)(2,1)}, u32[]{:S(2)}) copy-start(bf16[512,2048]{1,0:T(8,128)(2,1)} %param.26) | copy-start | bytes 6291460
  6.5 32.0 %copy-start.12 = (f32[128,8]{0,1:T(8,128)S(1)}, f32[128,8]{0,1:T(8,128)}, u32[]{:S(2)}) copy-start(f32[128,8]{0,1:T(8,128)} %param.24) | copy-start | bytes 12292
  6.5 61.1 %all-gather.14.cloned.1.call-start = ((), (), s32[]{:S(2)}) async-start(), calls=%async_computation.5 | async-start | bytes 2228224 | tf_op jit(solution)/shard_map/all_gather | solution.py:110
  7.3 95.8 %all-gather.8.cloned.1.call-start = ((), (), s32[]{:S(2)}) async-start(), calls=%async_computation.2 | async-start | bytes 2228224 | tf_op jit(solution)/shard_map/all_gather | solution.py:107
  8.0 137.0 %all-gather.12.cloned.1.call-start = ((), (), s32[]{:S(2)}) async-start(), calls=%async_computation.4 | async-start | bytes 2228224 | tf_op jit(solution)/shard_map/all_gather | solution.py:109
  9.7 177.8 %all-gather.10.cloned.1.call-start = ((), (), s32[]{:S(2)}) async-start(), calls=%async_computation.3 | async-start | bytes 2228224 | tf_op jit(solution)/shard_map/all_gather | solution.py:108
  10.3 204.2 %reduce-scatter.3.cloned.1.call-start = ((), (), s32[]{:S(2)}) async-start(), calls=%async_computation.6 | async-start | bytes 786432 | tf_op jit(solution)/shard_map/reduce_scatter | solution.py:116
  38.4 28.9 %copy-start.8 = (bf16[128,512]{1,0:T(8,128)(2,1)S(1)}, bf16[128,512]{1,0:T(8,128)(2,1)}, u32[]{:S(2)}) copy-start(bf16[128,512]{1,0:T(8,128)(2,1)} %param.18) | copy-start | bytes 393220
  67.6 77.4 %copy-start.13 = (bf16[128,512]{1,0:T(8,128)(2,1)S(1)}, bf16[128,512]{1,0:T(8,128)(2,1)}, u32[]{:S(2)}) copy-start(bf16[128,512]{1,0:T(8,128)(2,1)} %param.21) | copy-start | bytes 393220
  148.7 1.6 copy-start.7
  150.3 1.6 copy-start.6
  155.2 3.2 copy-start.2
  198.1 1.6 copy-start.5
  198.2 5.0 %copy-start.9 = (f32[3,2048]{1,0:T(4,128)S(1)}, f32[3,2048]{1,0:T(4,128)}, u32[]{:S(2)}) copy-start(f32[3,2048]{1,0:T(4,128)} %param.31) | copy-start | bytes 73732
  198.2 5.0 %copy-start.10 = (f32[3,2048]{1,0:T(4,128)S(1)}, f32[3,2048]{1,0:T(4,128)}, u32[]{:S(2)}) copy-start(f32[3,2048]{1,0:T(4,128)} %param.32) | copy-start | bytes 73732
  198.3 16.3 %copy-start.3 = (bf16[64,2048]{1,0:T(8,128)(2,1)S(1)}, bf16[64,2048]{1,0:T(8,128)(2,1)}, u32[]{:S(2)}) copy-start(bf16[64,2048]{1,0:T(8,128)(2,1)} %param.17) | copy-start | bytes 786436
  198.3 17.5 %copy-start.11 = (f32[2048]{0:T(1024)S(1)}, f32[2048]{0:T(1024)}, u32[]{:S(2)}) copy-start(f32[2048]{0:T(1024)} %param.28) | copy-start | bytes 24580
  201.1 89.8 %all-gather.18.cloned.1.call-start = ((), (), s32[]{:S(2)}) async-start(), calls=%async_computation.8 | async-start | bytes 8912896 | tf_op jit(solution)/shard_map/all_gather | solution.py:86
  201.6 164.3 %all-gather.16.cloned.1.call-start = ((), (), s32[]{:S(2)}) async-start(), calls=%async_computation.7 | async-start | bytes 8912896 | tf_op jit(solution)/shard_map/all_gather | solution.py:85
  202.4 242.1 %all-gather.20.cloned.1.call-start = ((), (), s32[]{:S(2)}) async-start(), calls=%async_computation.9 | async-start | bytes 8912896 | tf_op jit(solution)/shard_map/all_gather | solution.py:87
  203.1 260.6 %reduce-scatter.5.cloned.1.call-start = ((), (), s32[]{:S(2)}) async-start(), calls=%async_computation.10 | async-start | bytes 786432 | tf_op jit(solution)/shard_map/reduce_scatter | solution.py:144
  370.7 3.0 collective-permute-start
  375.9 87.8 %copy-start.4 = (bf16[64,2048]{1,0:T(8,128)(2,1)S(1)}, bf16[64,2048]{1,0:T(8,128)(2,1)}, u32[]{:S(2)}) copy-start(bf16[64,2048]{1,0:T(8,128)(2,1)} %reduce-scatter.3.cloned.1.call-done) | copy-start | bytes 786436
  444.5 21.0 %copy-start.1 = (bf16[512,2048]{1,0:T(8,128)(2,1)S(1)}, bf16[512,2048]{1,0:T(8,128)(2,1)}, u32[]{:S(2)}) copy-start(bf16[512,2048]{1,0:T(8,128)(2,1)} %param.26) | copy-start | bytes 6291460
Sparse Core Ops, SparseCore 0:
  9.5 49.7 all-gather.13
  61.4 41.5 all-gather.7
  105.2 39.7 all-gather.11
  147.0 40.5 all-gather.9
  201.2 13.3 reduce-scatter.2
  216.6 74.2 all-gather.17
  293.1 72.8 all-gather.15
  368.1 76.2 all-gather.19
  450.9 12.7 reduce-scatter.4
where the time goes:
time: 473 us; the launch traced here: 472 us
  waiting for transfers between devices  329 us (70%)
  blocking collectives  60.3 us (13%)
  matrix products  32.2 us (7%)
  local copies, waits for them, and re-layouts  22.4 us (5%)
  between operations  13.5 us (3%)
  other arithmetic  12.6 us (3%)
    all_gather x1, waiting for transfers between devices, body(): lax.all_gather(w_gate, 'sp', axis=0, tiled=True)  70.4 us
    all_gather x1, waiting for transfers between devices, body(): lax.all_gather(w_down, 'sp', axis=1, tiled=True)  68.5 us
    all_gather x1, waiting for transfers between devices, body(): lax.all_gather(w_up, 'sp', axis=0, tiled=True)  65.4 us
    all_gather x1, waiting for transfers between devices, body(): keys_l = lax.all_gather(k_large, 'sp', axis=0, tiled=True)  38 us
    all_gather x1, waiting for transfers between devices, body(): keys_s = lax.all_gather(k_small, 'sp', axis=0, tiled=True)  31.4 us
    all_gather x1, blocking collectives, body(): lax.all_gather(local_large, 'sp', axis=0, tiled=True)  27.1 us
    all_gather x1, waiting for transfers between devices, body(): values_s = lax.all_gather(v_small, 'sp', axis=0, tiled=True)  26 us
    all_gather x1, blocking collectives, body(): lax.all_gather(local_small, 'sp', axis=0, tiled=True)  24.5 us
  transfers between devices with their start and end apart: 10, of which 9 were waited for; matrix products, arithmetic and copies ran while one was open for 9% of the time, Pallas kernels for 0%

commit v1 on v0

--- a/solution.py
+++ b/solution.py
@@ -105,7 +105,13 @@
         empty_carry(rows, heads_large, queries_large.shape[2]),
     )
     keys_s = lax.all_gather(k_small, "sp", axis=0, tiled=True)
-    values_s = lax.all_gather(v_small, "sp", axis=0, tiled=True)
+    n_dev = lax.axis_size("sp")
+    held, shards = (v_small, [v_small])
+    for _ in range(n_dev - 1):
+        held = lax.ppermute(held, "sp", [(i_2, (i_2 + 1) % n_dev) for i_2 in range(n_dev)])
+        shards.insert(0, held)
+    merged = jnp.concatenate(shards, axis=0)
+    values_s = jnp.roll(merged, (lax.axis_index("sp") + 1) * v_small.shape[0], axis=0)
     keys_l = lax.all_gather(k_large, "sp", axis=0, tiled=True)
     values_l = lax.all_gather(v_large, "sp", axis=0, tiled=True)
     small = attend(start_carry[0], keys_s, values_s, queries_small, cum_small, every_small, qpos)

time: 473 us -> 492 us (1.040)
  local copies, waits for them, and re-layouts: 22.4 us -> 46.9 us
  waiting for transfers between devices: 329 us -> 323 us
    ppermute x0 -> x15, waiting for transfers between devices: none -> 87.5 us  [body(): lax.ppermute(held, 'sp', [(i_2, (i_2 + 1) % n_dev) for i_2 in range(n_dev)])]
    all_gather x1, waiting for transfers between devices: 38 us -> 0.01 us  [body(): keys_l = lax.all_gather(k_large, 'sp', axis=0, tiled=True)]
    all_gather x1, waiting for transfers between devices: 31.4 us -> 0.01 us  [body(): keys_s = lax.all_gather(k_small, 'sp', axis=0, tiled=True)]
    all_gather x1 -> x0, waiting for transfers between devices: 26 us -> none  [body(): values_s = lax.all_gather(v_small, 'sp', axis=0, tiled=True)]
    unnamed x31 -> x114, local copies, waits for them, and re-layouts: 7.27 us -> 27.5 us
    dynamic_slice x0 -> x2, local copies, waits for them, and re-layouts: none -> 5.54 us  [body(): jnp.roll(merged, (lax.axis_index('sp') + 1) * v_small.shape[0], axis=0)]
  transfers between devices with their start and end apart: 10 -> 24, of which waited for: 9 -> 18; matrix products, arithmetic and copies ran while one was open for 9% -> 14% of each run, Pallas kernels for 0% -> 0%
where the time goes in v1:
time: 492 us; the launch traced here: 491 us
  waiting for transfers between devices  323 us (66%)
  blocking collectives  57.5 us (12%)
  local copies, waits for them, and re-layouts  46.9 us (10%)
  matrix products  31.8 us (6%)
  other arithmetic  14.2 us (3%)
  between operations  14.2 us (3%)
    ppermute x15, waiting for transfers between devices, body(): lax.ppermute(held, 'sp', [(i_2, (i_2 + 1) % n_dev) for i_2 in range(n_dev)])  87.5 us
    all_gather x1, waiting for transfers between devices, body(): lax.all_gather(w_gate, 'sp', axis=0, tiled=True)  70.3 us
    all_gather x1, waiting for transfers between devices, body(): lax.all_gather(w_down, 'sp', axis=1, tiled=True)  68.6 us
    all_gather x1, waiting for transfers between devices, body(): lax.all_gather(w_up, 'sp', axis=0, tiled=True)  65.3 us
    unnamed x114, local copies, waits for them, and re-layouts  27.5 us
    all_gather x1, blocking collectives, body(): lax.all_gather(local_large, 'sp', axis=0, tiled=True)  25 us
    all_gather x1, blocking collectives, body(): lax.all_gather(local_small, 'sp', axis=0, tiled=True)  23.7 us
    reduce_scatter x1, waiting for transfers between devices, body(): lax.psum_scatter((first_part + jnp.dot(normed_large, w_out_large, preferr...  14.8 us
  transfers between devices with their start and end apart: 24, of which 18 were waited for; matrix products, arithmetic and copies ran while one was open for 14% of the time, Pallas kernels for 0%

profile of v1, /device:TPU:0, one launch (start us, length us, event | category | flops | bytes accessed | tf_op | source)
XLA Modules:
  0.0 490.9 jit_solution(10963269098566777868)
XLA Ops:
  9.6 7.8 %collective-permute-done = bf16[128,512]{1,0:T(8,128)(2,1)S(1)} collective-permute-done((bf16[128,512]{1,0:T(8,128)(2,1)}, bf16[128,512]{1,0:T(8,128)(2,1)S(1)}, u32[]{:S(2)}, u32[]{:S(2)}) %collective-permute-start) | collective-permute-done | bytes 131104 | tf_op jit(solution)/shard_map/ppermute | solution.py:111
  18.1 7.2 %collective-permute-done.1 = bf16[128,512]{1,0:T(8,128)(2,1)S(1)} collective-permute-done((bf16[128,512]{1,0:T(8,128)(2,1)S(1)}, bf16[128,512]{1,0:T(8,128)(2,1)S(1)}, u32[]{:S(2)}, u32[]{:S(2)}) %collective-permute-start.1) | collective-permute-done | bytes 131104 | tf_op jit(solution)/shard_map/ppermute | solution.py:111
  26.0 7.4 %collective-permute-done.2 = bf16[128,512]{1,0:T(8,128)(2,1)S(1)} collective-permute-done((bf16[128,512]{1,0:T(8,128)(2,1)S(1)}, bf16[128,512]{1,0:T(8,128)(2,1)S(1)}, u32[]{:S(2)}, u32[]{:S(2)}) %collective-permute-start.2) | collective-permute-done | bytes 131104 | tf_op jit(solution)/shard_map/ppermute | solution.py:111
  34.0 7.2 %collective-permute-done.3 = bf16[128,512]{1,0:T(8,128)(2,1)S(1)} collective-permute-done((bf16[128,512]{1,0:T(8,128)(2,1)S(1)}, bf16[128,512]{1,0:T(8,128)(2,1)S(1)}, u32[]{:S(2)}, u32[]{:S(2)}) %collective-permute-start.3) | collective-permute-done | bytes 131104 | tf_op jit(solution)/shard_map/ppermute | solution.py:111
  41.9 7.9 %collective-permute-done.4 = bf16[128,512]{1,0:T(8,128)(2,1)S(1)} collective-permute-done((bf16[128,512]{1,0:T(8,128)(2,1)S(1)}, bf16[128,512]{1,0:T(8,128)(2,1)S(1)}, u32[]{:S(2)}, u32[]{:S(2)}) %collective-permute-start.4) | collective-permute-done | bytes 131104 | tf_op jit(solution)/shard_map/ppermute | solution.py:111
  50.4 7.1 %collective-permute-done.5 = bf16[128,512]{1,0:T(8,128)(2,1)S(1)} collective-permute-done((bf16[128,512]{1,0:T(8,128)(2,1)S(1)}, bf16[128,512]{1,0:T(8,128)(2,1)S(1)}, u32[]{:S(2)}, u32[]{:S(2)}) %collective-permute-start.5) | collective-permute-done | bytes 131104 | tf_op jit(solution)/shard_map/ppermute | solution.py:111
  58.1 7.1 %collective-permute-done.6 = bf16[128,512]{1,0:T(8,128)(2,1)S(1)} collective-permute-done((bf16[128,512]{1,0:T(8,128)(2,1)S(1)}, bf16[128,512]{1,0:T(8,128)(2,1)S(1)}, u32[]{:S(2)}, u32[]{:S(2)}) %collective-permute-start.6) | collective-permute-done | bytes 131104 | tf_op jit(solution)/shard_map/ppermute | solution.py:111
  65.9 7.2 %collective-permute-done.7 = bf16[128,512]{1,0:T(8,128)(2,1)S(1)} collective-permute-done((bf16[128,512]{1,0:T(8,128)(2,1)S(1)}, bf16[128,512]{1,0:T(8,128)(2,1)S(1)}, u32[]{:S(2)}, u32[]{:S(2)}) %collective-permute-start.7) | collective-permute-done | bytes 131104 | tf_op jit(solution)/shard_map/ppermute | solution.py:111
  73.2 7.0 %collective-permute-done.8 = bf16[128,512]{1,0:T(8,128)(2,1)S(1)} collective-permute-done((bf16[128,512]{1,0:T(8,128)(2,1)S(1)}, bf16[128,512]{1,0:T(8,128)(2,1)S(1)}, u32[]{:S(2)}, u32[]{:S(2)}) %collective-permute-start.8) | collective-permute-done | bytes 131104 | tf_op jit(solution)/shard_map/ppermute | solution.py:111
  80.4 7.1 %collective-permute-done.9 = bf16[128,512]{1,0:T(8,128)(2,1)S(1)} collective-permute-done((bf16[128,512]{1,0:T(8,128)(2,1)S(1)}, bf16[128,512]{1,0:T(8,128)(2,1)S(1)}, u32[]{:S(2)}, u32[]{:S(2)}) %collective-permute-start.9) | collective-permute-done | bytes 131104 | tf_op jit(solution)/shard_map/ppermute | solution.py:111
  88.5 23.7 %all_gather.28 = f32[2048,8]{1,0:T(8,128)S(1)} all-gather(f32[128,8]{1,0:T(8,128)S(1)} %reduce_window_sum.44), channel_id=1, replica_groups=mesh['sp'=16,'tp'=2] {'sp'}, dimensions={0}, use_global_device_ids=true | all-gather | bytes 69632 | tf_op jit(solution)/shard_map/all_gather | solution.py:92
  112.7 8.1 %collective-permute-done.11 = bf16[128,512]{1,0:T(8,128)(2,1)} collective-permute-done((bf16[128,512]{1,0:T(8,128)(2,1)S(1)}, bf16[128,512]{1,0:T(8,128)(2,1)}, u32[]{:S(2)}, u32[]{:S(2)}) %collective-permute-start.11) | collective-permute-done | bytes 131104 | tf_op jit(solution)/shard_map/ppermute | solution.py:111
  123.2 25.0 %all_gather.30 = f32[2048,4]{1,0:T(8,128)S(1)} all-gather(f32[128,4]{1,0:T(8,128)} %reduce_window_sum.46), channel_id=1, replica_groups=mesh['sp'=16,'tp'=2] {'sp'}, dimensions={0}, use_global_device_ids=true | all-gather | bytes 34816 | tf_op jit(solution)/shard_map/all_gather | solution.py:93
  149.1 6.4 %collective-permute-done.13 = bf16[128,512]{1,0:T(8,128)(2,1)} collective-permute-done((bf16[128,512]{1,0:T(8,128)(2,1)}, bf16[128,512]{1,0:T(8,128)(2,1)}, u32[]{:S(2)}, u32[]{:S(2)}) %collective-permute-start.13) | collective-permute-done | bytes 131104 | tf_op jit(solution)/shard_map/ppermute | solution.py:111
  183.0 4.1 copy.35
  187.1 4.0 copy.36
  191.1 3.8 fusion.47
  195.0 3.4 fusion.4
  198.5 3.1 fusion.2
  201.6 3.3 multiply_reduce_fusion.2
  205.7 4.0 copy.52
  209.7 3.9 multiply_reduce_fusion.1
  218.5 14.8 %reduce-scatter.3.cloned.1.call-done = bf16[64,2048]{1,0:T(8,128)(2,1)} async-done(((bf16[128,2048]{1,0:T(8,128)(2,1)}), bf16[64,2048]{1,0:T(8,128)(2,1)}) %reduce-scatter.3.cloned.1.call-update) | async-done | bytes 262160 | tf_op jit(solution)/shard_map/reduce_scatter | solution.py:122
  235.6 8.8 %all_gather.32 = bf16[128,2048]{1,0:T(8,128)(2,1)S(1)} all-gather(bf16[64,2048]{1,0:T(8,128)(2,1)S(1)} %multiply_convert_fusion), channel_id=1, replica_groups=mesh['sp'=16,'tp'=2] {'tp'}, dimensions={0}, use_global_device_ids=true | all-gather | bytes 786432 | tf_op jit(solution)/shard_map/all_gather | solution.py:135
  244.3 65.3 %all-gather.15.cloned.1.call-done = bf16[2048,2048]{1,0:T(8,128)(2,1)} async-done(((bf16[128,2048]{1,0:T(8,128)(2,1)}), bf16[2048,2048]{1,0:T(8,128)(2,1)}) %all-gather.15.cloned.1.call-update) | async-done | bytes 8388624 | tf_op jit(solution)/shard_map/all_gather | solution.py:86
  309.7 4.6 convolution_convert_fusion.1
  314.3 70.3 %all-gather.13.cloned.1.call-done = bf16[2048,2048]{1,0:T(8,128)(2,1)} async-done(((bf16[128,2048]{1,0:T(8,128)(2,1)}), bf16[2048,2048]{1,0:T(8,128)(2,1)}) %all-gather.13.cloned.1.call-update) | async-done | bytes 8388624 | tf_op jit(solution)/shard_map/all_gather | solution.py:85
  384.6 4.6 convolution_convert_fusion.2
  389.3 2.2 collective-permute-start.15
  394.5 68.6 %all-gather.17.cloned.1.call-done = bf16[2048,2048]{1,0:T(8,128)(2,1)} async-done(((bf16[2048,128]{1,0:T(8,128)(2,1)}), bf16[2048,2048]{1,0:T(8,128)(2,1)}) %all-gather.17.cloned.1.call-update) | async-done | bytes 8388624 | tf_op jit(solution)/shard_map/all_gather | solution.py:87
  463.1 6.3 %convolution_convert_fusion = bf16[128,2048]{1,0:T(8,128)(2,1)} fusion(bf16[2048,2048]{1,0:T(8,128)(2,1)} %all-gather.17.cloned.1.call-done, f32[128,4096]{1,0:T(8,128)} %fusion.15), kind=kOutput, calls=%fused_computation.16 | convolution fusion | flops 1075576832 | bytes 11010048 | tf_op jit(solution)/shard_map/dot_general | solution.py:151
  469.4 13.0 %reduce-scatter.5.cloned.1.call-done = bf16[64,2048]{1,0:T(8,128)(2,1)} async-done(((bf16[128,2048]{1,0:T(8,128)(2,1)}), bf16[64,2048]{1,0:T(8,128)(2,1)}) %reduce-scatter.5.cloned.1.call-update) | async-done | bytes 262160 | tf_op jit(solution)/shard_map/reduce_scatter | solution.py:150
  (190 shorter events, 52.4 us)
Async XLA Ops:
  6.5 207.1 %copy-start = (bf16[512,2048]{1,0:T(8,128)(2,1)S(1)}, bf16[512,2048]{1,0:T(8,128)(2,1)}, u32[]{:S(2)}) copy-start(bf16[512,2048]{1,0:T(8,128)(2,1)} %param.26) | copy-start | bytes 6291460
  6.5 114.3 %copy-start.38 = (f32[128,4]{0,1:T(4,128)S(1)}, f32[128,4]{0,1:T(4,128)}, u32[]{:S(2)}) copy-start(f32[128,4]{0,1:T(4,128)} %param.25) | copy-start | bytes 6148
  6.5 180.6 %all-gather.7.cloned.1.call-start = ((), (), s32[]{:S(2)}) async-start(), calls=%async_computation.2 | async-start | bytes 2228224 | tf_op jit(solution)/shard_map/all_gather | solution.py:107
  7.3 183.8 %all-gather.9.cloned.1.call-start = ((), (), s32[]{:S(2)}) async-start(), calls=%async_computation.3 | async-start | bytes 2228224 | tf_op jit(solution)/shard_map/all_gather | solution.py:115
  9.0 196.7 %all-gather.11.cloned.1.call-start = ((), (), s32[]{:S(2)}) async-start(), calls=%async_computation.4 | async-start | bytes 2228224 | tf_op jit(solution)/shard_map/all_gather | solution.py:116
  9.0 8.4 %collective-permute-start = (bf16[128,512]{1,0:T(8,128)(2,1)}, bf16[128,512]{1,0:T(8,128)(2,1)S(1)}, u32[]{:S(2)}, u32[]{:S(2)}) collective-permute-start(bf16[128,512]{1,0:T(8,128)(2,1)} %param.20), channel_id=1, source_target_pairs={{0,2},{2,4},{4,6},{6,8},{8,10},{10,12},{12,14},{14,16},{16,18},{18... | collective-permute-start | bytes 393224 | tf_op jit(solution)/shard_map/ppermute | solution.py:111
  18.1 7.2 %collective-permute-start.1 = (bf16[128,512]{1,0:T(8,128)(2,1)S(1)}, bf16[128,512]{1,0:T(8,128)(2,1)S(1)}, u32[]{:S(2)}, u32[]{:S(2)}) collective-permute-start(bf16[128,512]{1,0:T(8,128)(2,1)S(1)} %collective-permute-done), channel_id=1, source_target_pairs={{0,2},{2,4},{4,6},{6,8},{8,10},{10,12},{12,14},{14,16},{16,18},{18... | collective-permute-start | bytes 393224 | tf_op jit(solution)/shard_map/ppermute | solution.py:111
  26.0 7.4 %collective-permute-start.2 = (bf16[128,512]{1,0:T(8,128)(2,1)S(1)}, bf16[128,512]{1,0:T(8,128)(2,1)S(1)}, u32[]{:S(2)}, u32[]{:S(2)}) collective-permute-start(bf16[128,512]{1,0:T(8,128)(2,1)S(1)} %collective-permute-done.1), channel_id=1, source_target_pairs={{0,2},{2,4},{4,6},{6,8},{8,10},{10,12},{12,14},{14,16},{16,18},{18... | collective-permute-start | bytes 393224 | tf_op jit(solution)/shard_map/ppermute | solution.py:111
  34.0 7.2 %collective-permute-start.3 = (bf16[128,512]{1,0:T(8,128)(2,1)S(1)}, bf16[128,512]{1,0:T(8,128)(2,1)S(1)}, u32[]{:S(2)}, u32[]{:S(2)}) collective-permute-start(bf16[128,512]{1,0:T(8,128)(2,1)S(1)} %collective-permute-done.2), channel_id=1, source_target_pairs={{0,2},{2,4},{4,6},{6,8},{8,10},{10,12},{12,14},{14,16},{16,18},{18... | collective-permute-start | bytes 393224 | tf_op jit(solution)/shard_map/ppermute | solution.py:111
  41.9 7.9 %collective-permute-start.4 = (bf16[128,512]{1,0:T(8,128)(2,1)S(1)}, bf16[128,512]{1,0:T(8,128)(2,1)S(1)}, u32[]{:S(2)}, u32[]{:S(2)}) collective-permute-start(bf16[128,512]{1,0:T(8,128)(2,1)S(1)} %collective-permute-done.3), channel_id=1, source_target_pairs={{0,2},{2,4},{4,6},{6,8},{8,10},{10,12},{12,14},{14,16},{16,18},{18... | collective-permute-start | bytes 393224 | tf_op jit(solution)/shard_map/ppermute | solution.py:111
  50.4 7.1 %collective-permute-start.5 = (bf16[128,512]{1,0:T(8,128)(2,1)S(1)}, bf16[128,512]{1,0:T(8,128)(2,1)S(1)}, u32[]{:S(2)}, u32[]{:S(2)}) collective-permute-start(bf16[128,512]{1,0:T(8,128)(2,1)S(1)} %collective-permute-done.4), channel_id=1, source_target_pairs={{0,2},{2,4},{4,6},{6,8},{8,10},{10,12},{12,14},{14,16},{16,18},{18... | collective-permute-start | bytes 393224 | tf_op jit(solution)/shard_map/ppermute | solution.py:111
  58.1 7.1 %collective-permute-start.6 = (bf16[128,512]{1,0:T(8,128)(2,1)S(1)}, bf16[128,512]{1,0:T(8,128)(2,1)S(1)}, u32[]{:S(2)}, u32[]{:S(2)}) collective-permute-start(bf16[128,512]{1,0:T(8,128)(2,1)S(1)} %collective-permute-done.5), channel_id=1, source_target_pairs={{0,2},{2,4},{4,6},{6,8},{8,10},{10,12},{12,14},{14,16},{16,18},{18... | collective-permute-start | bytes 393224 | tf_op jit(solution)/shard_map/ppermute | solution.py:111
  65.9 7.2 %collective-permute-start.7 = (bf16[128,512]{1,0:T(8,128)(2,1)S(1)}, bf16[128,512]{1,0:T(8,128)(2,1)S(1)}, u32[]{:S(2)}, u32[]{:S(2)}) collective-permute-start(bf16[128,512]{1,0:T(8,128)(2,1)S(1)} %collective-permute-done.6), channel_id=1, source_target_pairs={{0,2},{2,4},{4,6},{6,8},{8,10},{10,12},{12,14},{14,16},{16,18},{18... | collective-permute-start | bytes 393224 | tf_op jit(solution)/shard_map/ppermute | solution.py:111
  73.1 39.5 %copy-start.24 = (bf16[128,512]{1,0:T(8,128)(2,1)}, bf16[128,512]{1,0:T(8,128)(2,1)S(1)}, u32[]{:S(2)}) copy-start(bf16[128,512]{1,0:T(8,128)(2,1)S(1)} %collective-permute-done.7) | copy-start | bytes 393220
  73.1 7.1 %collective-permute-start.8 = (bf16[128,512]{1,0:T(8,128)(2,1)S(1)}, bf16[128,512]{1,0:T(8,128)(2,1)S(1)}, u32[]{:S(2)}, u32[]{:S(2)}) collective-permute-start(bf16[128,512]{1,0:T(8,128)(2,1)S(1)} %collective-permute-done.7), channel_id=1, source_target_pairs={{0,2},{2,4},{4,6},{6,8},{8,10},{10,12},{12,14},{14,16},{16,18},{18... | collective-permute-start | bytes 393224 | tf_op jit(solution)/shard_map/ppermute | solution.py:111
  73.1 160.2 %reduce-scatter.3.cloned.1.call-start = ((), (), s32[]{:S(2)}) async-start(), calls=%async_computation.5 | async-start | bytes 786432 | tf_op jit(solution)/shard_map/reduce_scatter | solution.py:122
  80.2 32.4 %copy-start.26 = (bf16[128,512]{1,0:T(8,128)(2,1)}, bf16[128,512]{1,0:T(8,128)(2,1)S(1)}, u32[]{:S(2)}) copy-start(bf16[128,512]{1,0:T(8,128)(2,1)S(1)} %collective-permute-done.8) | copy-start | bytes 393220
  80.2 7.3 %collective-permute-start.9 = (bf16[128,512]{1,0:T(8,128)(2,1)S(1)}, bf16[128,512]{1,0:T(8,128)(2,1)S(1)}, u32[]{:S(2)}, u32[]{:S(2)}) collective-permute-start(bf16[128,512]{1,0:T(8,128)(2,1)S(1)} %collective-permute-done.8), channel_id=1, source_target_pairs={{0,2},{2,4},{4,6},{6,8},{8,10},{10,12},{12,14},{14,16},{16,18},{18... | collective-permute-start | bytes 393224 | tf_op jit(solution)/shard_map/ppermute | solution.py:111
  87.5 25.1 %copy-start.28 = (bf16[128,512]{1,0:T(8,128)(2,1)}, bf16[128,512]{1,0:T(8,128)(2,1)S(1)}, u32[]{:S(2)}) copy-start(bf16[128,512]{1,0:T(8,128)(2,1)S(1)} %collective-permute-done.9) | copy-start | bytes 393220
  87.5 24.7 %collective-permute-start.10 = (bf16[128,512]{1,0:T(8,128)(2,1)S(1)}, bf16[128,512]{1,0:T(8,128)(2,1)S(1)}, u32[]{:S(2)}, u32[]{:S(2)}) collective-permute-start(bf16[128,512]{1,0:T(8,128)(2,1)S(1)} %collective-permute-done.9), channel_id=1, source_target_pairs={{0,2},{2,4},{4,6},{6,8},{8,10},{10,12},{12,14},{14,16},{16,18},{18... | collective-permute-start | bytes 393224 | tf_op jit(solution)/shard_map/ppermute | solution.py:111
  112.2 44.9 %copy-start.30 = (bf16[128,512]{1,0:T(8,128)(2,1)}, bf16[128,512]{1,0:T(8,128)(2,1)S(1)}, u32[]{:S(2)}) copy-start(bf16[128,512]{1,0:T(8,128)(2,1)S(1)} %collective-permute-done.10) | copy-start | bytes 393220
  112.2 8.6 %collective-permute-start.11 = (bf16[128,512]{1,0:T(8,128)(2,1)S(1)}, bf16[128,512]{1,0:T(8,128)(2,1)}, u32[]{:S(2)}, u32[]{:S(2)}) collective-permute-start(bf16[128,512]{1,0:T(8,128)(2,1)S(1)} %collective-permute-done.10), channel_id=1, source_target_pairs={{0,2},{2,4},{4,6},{6,8},{8,10},{10,12},{12,14},{14,16},{16,18},{18... | collective-permute-start | bytes 393224 | tf_op jit(solution)/shard_map/ppermute | solution.py:111
  120.8 27.4 %collective-permute-start.12 = (bf16[128,512]{1,0:T(8,128)(2,1)}, bf16[128,512]{1,0:T(8,128)(2,1)}, u32[]{:S(2)}, u32[]{:S(2)}) collective-permute-start(bf16[128,512]{1,0:T(8,128)(2,1)} %collective-permute-done.11), channel_id=1, source_target_pairs={{0,2},{2,4},{4,6},{6,8},{8,10},{10,12},{12,14},{14,16},{16,18},{18... | collective-permute-start | bytes 393224 | tf_op jit(solution)/shard_map/ppermute | solution.py:111
  148.2 7.4 %collective-permute-start.13 = (bf16[128,512]{1,0:T(8,128)(2,1)}, bf16[128,512]{1,0:T(8,128)(2,1)}, u32[]{:S(2)}, u32[]{:S(2)}) collective-permute-start(bf16[128,512]{1,0:T(8,128)(2,1)} %collective-permute-done.12), channel_id=1, source_target_pairs={{0,2},{2,4},{4,6},{6,8},{8,10},{10,12},{12,14},{14,16},{16,18},{18... | collective-permute-start | bytes 393224 | tf_op jit(solution)/shard_map/ppermute | solution.py:111
  155.6 8.0 %collective-permute-start.14 = (bf16[128,512]{1,0:T(8,128)(2,1)}, bf16[128,512]{1,0:T(8,128)(2,1)}, u32[]{:S(2)}, u32[]{:S(2)}) collective-permute-start(bf16[128,512]{1,0:T(8,128)(2,1)} %collective-permute-done.13), channel_id=1, source_target_pairs={{0,2},{2,4},{4,6},{6,8},{8,10},{10,12},{12,14},{14,16},{16,18},{18... | collective-permute-start | bytes 393224 | tf_op jit(solution)/shard_map/ppermute | solution.py:111
  216.5 93.1 %all-gather.15.cloned.1.call-start = ((), (), s32[]{:S(2)}) async-start(), calls=%async_computation.7 | async-start | bytes 8912896 | tf_op jit(solution)/shard_map/all_gather | solution.py:86
  217.1 167.5 %all-gather.13.cloned.1.call-start = ((), (), s32[]{:S(2)}) async-start(), calls=%async_computation.6 | async-start | bytes 8912896 | tf_op jit(solution)/shard_map/all_gather | solution.py:85
  217.7 245.4 %all-gather.17.cloned.1.call-start = ((), (), s32[]{:S(2)}) async-start(), calls=%async_computation.8 | async-start | bytes 8912896 | tf_op jit(solution)/shard_map/all_gather | solution.py:87
  218.4 263.9 %reduce-scatter.5.cloned.1.call-start = ((), (), s32[]{:S(2)}) async-start(), calls=%async_computation.9 | async-start | bytes 786432 | tf_op jit(solution)/shard_map/reduce_scatter | solution.py:150
  389.3 3.0 collective-permute-start.15
  394.5 87.9 %copy-start.5 = (bf16[64,2048]{1,0:T(8,128)(2,1)S(1)}, bf16[64,2048]{1,0:T(8,128)(2,1)}, u32[]{:S(2)}) copy-start(bf16[64,2048]{1,0:T(8,128)(2,1)} %reduce-scatter.3.cloned.1.call-done) | copy-start | bytes 786436
  463.1 21.0 %copy-start.1 = (bf16[512,2048]{1,0:T(8,128)(2,1)S(1)}, bf16[512,2048]{1,0:T(8,128)(2,1)}, u32[]{:S(2)}) copy-start(bf16[512,2048]{1,0:T(8,128)(2,1)} %param.26) | copy-start | bytes 6291460
  (32 other events, 314.1 us)
Sparse Core Ops, SparseCore 0:
  9.5 45.7 all-gather.6
  57.4 42.6 all-gather.8
  102.2 43.4 all-gather.10
  216.6 16.6 reduce-scatter.2
  235.3 74.2 all-gather.14
  311.7 72.8 all-gather.12
  386.7 76.2 all-gather.16
  469.5 12.7 reduce-scatter.4
